TPU v7x, 512 devices: a whole 4x4x16 slice. The times are simulated.
512 devices in a mesh: sp: 32 (over z, core), tp: 16 (over y, x).
Axes of the slice: x: 4, y: 4, z: 16, core: 2. Of those that a mesh axis runs over, the one named last changes fastest.
Arguments:
- cotangent: bfloat16 [4096, 2048], P('sp'), may hold values from -6 to 6
- normed: bfloat16 [4096, 2048], P('sp'), may hold values from -6 to 6
- inverse_root_mean_square: float32 [4096], P('sp'), may hold values from 0.5 to 2
- expert_norm_scale: float32 [2048], replicated, may hold values from 0.1 to 1.9
- routes: int32 [4096, 2], P('sp'), may hold values from 0 to 31, all different within a row; in each aligned block of 128 rows (0 to 127, 128 to 255, ...) at most 16 rows name the same one
- route_probability_weight: float32 [4096, 2], P('sp'), may hold values from 0.2 to 1
- gate_weight: bfloat16 [32, 2048, 2048], P('sp', None, 'tp'), may hold values from -0.125 to 0.125
- up_weight: bfloat16 [32, 2048, 2048], P('sp', None, 'tp'), may hold values from -0.125 to 0.125
- down_weight: bfloat16 [32, 2048, 2048], P('sp', 'tp'), may hold values from -0.125 to 0.125
- recurrence_input: bfloat16 [4096, 1024], P('sp', 'tp'), may hold values from -6 to 6
- recurrence_gate_logits: bfloat16 [4096, 1024], P('sp', 'tp'), may hold values from -6 to 6
- input_gate_logits: bfloat16 [4096, 1024], P('sp', 'tp'), may hold values from -6 to 6
- channel_decay_weight: float32 [1024], P('tp'), may hold values from 3 to 20
- extra_log_decay: float32 [4096, 1024], P('sp', 'tp'), may hold values from -1 to 0
- output_matrix: bfloat16 [2048, 1024], P(None, 'tp'), may hold values from -0.1875 to 0.1875
Outputs:
- grad_gate: bfloat16 [32, 2048, 2048], P('sp', None, 'tp')
- grad_up: bfloat16 [32, 2048, 2048], P('sp', None, 'tp')
- grad_down: bfloat16 [32, 2048, 2048], P('sp', 'tp')
- grad_out_weight: float32 [2048, 1024], P('sp', 'tp')
- grad_rec_input: float32 [4096, 1024], P('sp', 'tp')
- grad_decay_gate: float32 [4096, 1024], P('sp', 'tp')
- grad_input_gate: float32 [4096, 1024], P('sp', 'tp')
Inputs may be any that keep to these rules, and one draw needn't show every extreme that they name: `routes`: each row names 2 different experts; among the rows of one device no expert is named more than 16 times.
All inputs are finite; a program needn't handle non-finite values.
Results may differ from a plain program's by a relative error of at most 0.025.
Values may be sent and summed in bfloat16 or wider, within the bound.
A program may use at most 64 MiB of HBM per device.

v0:
```python
import jax
import jax.numpy as jnp
from jax import lax
from jax.sharding import Mesh
from jax.sharding import PartitionSpec as P

TP = ("tp_0", "tp_1")


def side_by_side(arrays, axis, split_dim, concat_dim, along):
    both = jnp.concatenate(arrays, axis=along)
    filled, at, gathered = (
        lax.all_to_all(both, axis, split_axis=split_dim, concat_axis=concat_dim, tiled=True),
        0,
        [],
    )
    for a in arrays:
        gathered.append(lax.slice_in_dim(filled, at, at + a.shape[along], axis=along))
        at += a.shape[along]
    return tuple(gathered)


def in_blocks(value, dim, count):
    dims = value.shape
    parts = value.reshape(*dims[:dim], count, dims[dim] // count, *dims[dim + 1 :])
    return jnp.moveaxis(parts, dim, 0)


def sum_at_owner(value, axis, dim):
    parts = in_blocks(value, dim, lax.axis_size(axis))
    arrived = lax.all_to_all(parts, axis, split_axis=0, concat_axis=0, tiled=True)
    return arrived.astype(jnp.float32).sum(axis=0)


def over_axes(value, axes):
    for axis in axes:
        value = lax.psum(value, axis)
    return value


def in_order(parts, dim):
    parts = jnp.moveaxis(parts, 0, dim)
    dims = parts.shape
    return parts.reshape(*dims[:dim], dims[dim] * dims[dim + 1], *dims[dim + 2 :])


def sent_to_all(value, axis):
    count = lax.axis_size(axis)
    return lax.all_to_all(
        jnp.broadcast_to(value[None], (count, *value.shape)), axis, 0, 0, tiled=True
    )


def gathered_copies(value, axis, dim):
    return in_order(sent_to_all(value, axis), dim)


def gathered_once(value, axis):
    leaves = jax.tree.leaves(value)
    sequence = sorted(range(len(leaves)), key=lambda k: -leaves[k].size)
    width = (1, *leaves[sequence[0]].shape)[-1]
    lines = [
        jnp.pad(leaves[k].reshape(-1), (0, -leaves[k].size % width)).reshape(-1, width)
        for k in sequence
    ]
    both, at, found = (sent_to_all(jnp.concatenate(lines), axis), 0, {})
    for k, line in zip(sequence, lines):
        section = both[:, at : at + len(line)].reshape(len(both), -1)
        found[k] = section[:, : leaves[k].size].reshape(-1, *leaves[k].shape)
        at += len(line)
    numbers = iter(range(len(leaves)))
    return jax.tree.map(lambda _: found[next(numbers)], value)


def joined_by_halves(pieces, combine):
    while len(jax.tree.leaves(pieces)[0]) > 1:
        pieces = jax.vmap(combine)(
            *(jax.tree.map(lambda part: part[side::2], pieces) for side in (0, 1))
        )
    return jax.tree.map(lambda part: part[0], pieces)


def entering(value, axis, combine, identity, reverse):
    count, here = (lax.axis_size(axis), lax.axis_index(axis))
    passed = jnp.arange(count) > here if reverse else jnp.arange(count) < here

    def kept(part, zero, own):
        part = jnp.where(
            passed.reshape(-1, *(1 for _ in own.shape)), part, jnp.asarray(zero, own.dtype)
        )
        return part[::-1] if reverse else part

    pieces = gathered_once(value, axis)
    return joined_by_halves(jax.tree.map(kept, pieces, identity, value), combine)


def link(earlier, later):
    return (earlier[0] * later[0], later[0] * earlier[1] + later[1])


def shards(
    cotangent,
    normed,
    inverse_root_mean_square,
    expert_norm_scale,
    routes,
    route_probability_weight,
    gate_weight,
    up_weight,
    down_weight,
    recurrence_input,
    recurrence_gate_logits,
    input_gate_logits,
    channel_decay_weight,
    extra_log_decay,
    output_matrix,
):
    tok_rows, features = normed.shape
    groups = lax.axis_size("sp")
    picks = routes.shape[1]
    capacity = 2 * picks * tok_rows // groups
    rowdims = (((0,), (0,)), ((), ()))
    coldims = (((1,), (1,)), ((), ()))
    chosen = routes.reshape(-1)
    member = (chosen[:, None] == jnp.arange(groups, dtype=jnp.int32)[None, :]).astype(jnp.int32)
    ranking = jnp.sum((jnp.cumsum(member, axis=0) - member) * member, axis=1)
    landing = chosen * capacity + ranking
    scaled = (
        route_probability_weight[:, :, None] * cotangent[:, None, :].astype(jnp.float32)
    ).astype(jnp.bfloat16)
    scaled = scaled.reshape(tok_rows * picks, features)
    copies = jnp.repeat(normed, picks, axis=0)
    grad_send = jnp.zeros((groups * capacity, features), jnp.bfloat16).at[landing].set(scaled)
    token_send = jnp.zeros((groups * capacity, features), jnp.bfloat16).at[landing].set(copies)
    grad_recv, token_recv = side_by_side((grad_send, token_send), "sp", 0, 0, 1)
    gate_w = gate_weight[0]
    up_w = up_weight[0]
    down_w = down_weight[0]
    gate_pre = jnp.dot(token_recv, gate_w, preferred_element_type=jnp.float32)
    up_pre = jnp.dot(token_recv, up_w, preferred_element_type=jnp.float32)
    sigma = jax.nn.sigmoid(gate_pre)
    swish = gate_pre * sigma
    active = (swish * up_pre).astype(jnp.bfloat16)
    d_active = lax.dot_general(grad_recv, down_w, coldims, preferred_element_type=jnp.float32)
    d_gate = (d_active * up_pre * sigma * (1.0 + gate_pre * (1.0 - sigma))).astype(jnp.bfloat16)
    d_up = (d_active * swish).astype(jnp.bfloat16)
    grad_down = lax.dot_general(
        active, grad_recv, rowdims, preferred_element_type=jnp.float32
    ).astype(jnp.bfloat16)
    grad_gate = lax.dot_general(
        token_recv, d_gate, rowdims, preferred_element_type=jnp.float32
    ).astype(jnp.bfloat16)
    grad_up = lax.dot_general(token_recv, d_up, rowdims, preferred_element_type=jnp.float32).astype(
        jnp.bfloat16
    )
    partial_rows = lax.dot_general(d_gate, gate_w, coldims, preferred_element_type=jnp.float32)
    partial_rows = partial_rows + lax.dot_general(
        d_up, up_w, coldims, preferred_element_type=jnp.float32
    )
    shared = sum_at_owner(partial_rows.astype(jnp.bfloat16), TP, 1).astype(jnp.bfloat16)
    returned = lax.all_to_all(shared, "sp", split_axis=0, concat_axis=0, tiled=True)
    slice_width = returned.shape[1]
    offset = lax.axis_index(TP) * slice_width
    gain_part = lax.dynamic_slice_in_dim(expert_norm_scale, offset, slice_width, 0)
    normed_part = lax.dynamic_slice_in_dim(normed, offset, slice_width, 1)
    cot_part = lax.dynamic_slice_in_dim(cotangent, offset, slice_width, 1)
    d_norm = jnp.sum(
        returned[landing].astype(jnp.float32).reshape(tok_rows, picks, slice_width), axis=1
    )
    nhat = normed_part.astype(jnp.float32) / gain_part[None, :]
    gained = gain_part[None, :] * d_norm
    stat = over_axes(jnp.sum(gained * nhat, axis=1), TP)[:, None] / features
    mix_part = (
        cot_part.astype(jnp.float32) + inverse_root_mean_square[:, None] * (gained - nhat * stat)
    ).astype(jnp.bfloat16)
    d_mix = gathered_copies(mix_part, TP, 1)
    retention_factor = jax.nn.sigmoid(recurrence_gate_logits.astype(jnp.float32))
    admit = jax.nn.sigmoid(input_gate_logits.astype(jnp.float32))
    signal = recurrence_input.astype(jnp.float32)
    decay_speed = jax.nn.softplus(-channel_decay_weight)
    log_retention = -8.0 * retention_factor * decay_speed[None, :] + extra_log_decay
    keep = jnp.exp(log_retention)
    scale_in = jnp.sqrt(-jnp.expm1(2.0 * log_retention))
    driven = scale_in * admit * signal
    channels = keep.shape[1]
    identity = (jnp.ones((channels,), jnp.float32), jnp.zeros((channels,), jnp.float32))
    keep_cum, state_loc = lax.associative_scan(link, (keep, driven), axis=0)
    _, state_in = entering((keep_cum[-1], state_loc[-1]), "sp", link, identity, False)
    state = state_loc + keep_cum * state_in[None, :]
    hidden = state.astype(jnp.bfloat16)
    state_prev = jnp.concatenate([state_in[None, :], state[:-1]], axis=0)
    grad_out_weight = sum_at_owner(
        lax.dot_general(d_mix, hidden, rowdims, preferred_element_type=jnp.float32).astype(
            jnp.bfloat16
        ),
        "sp",
        0,
    )
    d_state = jnp.dot(d_mix, output_matrix, preferred_element_type=jnp.float32)
    keep_next = jnp.concatenate([keep[1:], jnp.ones((1, channels), jnp.float32)], axis=0)
    tail_keep, grad_loc = lax.associative_scan(link, (keep_next, d_state), reverse=True, axis=0)
    block_map = (keep[0] * tail_keep[0], keep[0] * grad_loc[0])
    _, grad_enter = entering(block_map, "sp", link, identity, True)
    total = grad_loc + tail_keep * grad_enter[None, :]
    grad_rec_input = total * scale_in * admit
    grad_input_gate = total * scale_in * signal * admit * (1.0 - admit)
    d_log = total * state_prev * keep - total * admit * signal * keep * keep / scale_in
    grad_decay_gate = (
        d_log * (-8.0 * decay_speed[None, :]) * retention_factor * (1.0 - retention_factor)
    )
    return (
        grad_gate[None],
        grad_up[None],
        grad_down[None],
        grad_out_weight,
        grad_rec_input,
        grad_decay_gate,
        grad_input_gate,
    )


def solution(mesh):
    finer = Mesh(mesh.devices.reshape(mesh.shape["sp"], 4, 4), ("sp", "tp_0", "tp_1"))
    placed = (
        P("sp", None),
        P("sp", None),
        P("sp"),
        P(),
        P("sp", None),
        P("sp", None),
        P("sp", None, TP),
        P("sp", None, TP),
        P("sp", TP, None),
        P("sp", TP),
        P("sp", TP),
        P("sp", TP),
        P(TP),
        P("sp", TP),
        P(None, TP),
    )
    return jax.shard_map(
        shards,
        mesh=finer,
        in_specs=placed,
        out_specs=(
            P("sp", None, TP),
            P("sp", None, TP),
            P("sp", TP, None),
            P("sp", TP),
            P("sp", TP),
            P("sp", TP),
            P("sp", TP),
        ),
        check_vma=False,
    )
```

profile of v0, /device:TPU:1, one launch (start us, length us, event | category | flops | bytes accessed | tf_op | source)
XLA Modules:
  0.0 428.7 jit_solution(14606756271678646964)
XLA Ops:
  0.7 0.8 broadcast_multiply_fusion
  1.4 0.8 copy.99
  3.6 1.7 broadcast_in_dim.73
  5.3 1.2 reshape.155
  6.5 2.4 mul.410
  8.9 2.7 mul.411
  12.0 4.4 %scatter_custom_fusion.1 = bf16[512,2048]{1,0:T(8,128)(2,1)} fusion(s32[256]{0:T(256)S(1)} %bitcast.130, bf16[256,2048]{1,0:T(8,128)(2,1)} %reshape.155, bf16[]{:T(256)} %constant.16.clone.1), kind=kCustom, calls=%fused_computation.27 | custom fusion | bytes 2097664 | tf_op jit(solution)/shard_map/scatter | solution.py:134
  16.4 3.8 scatter_custom_fusion
  20.2 2.7 pad_maximum_fusion
  22.9 207.4 %all_to_all.49 = bf16[32,16,4096]{2,1,0:T(8,128)(2,1)S(1)} all-to-all(bf16[32,16,4096]{2,1,0:T(8,128)(2,1)S(1)} %bitcast.99), channel_id=1, replica_groups=mesh['sp'=32,'tp_0'=4,'tp_1'=4] {'sp'}, dimensions={0} | all-to-all | bytes 8388608 | tf_op jit(solution)/shard_map/all_to_all | solution.py:13
  230.2 0.7 fusion.9
  231.0 0.7 copy-done.4
  231.6 0.7 fusion.11
  233.0 0.7 multiply_convert_fusion.3
  233.7 0.7 fusion.18
  234.4 0.7 fusion.6
  235.7 34.0 %all_to_all.50 = bf16[16,512,128]{2,1,0:T(8,128)(2,1)S(1)} all-to-all(bf16[16,512,128]{2,1,0:T(8,128)(2,1)S(1)} %bitcast.100), channel_id=1, replica_groups=mesh['sp'=32,'tp_0'=4,'tp_1'=4] {'tp_0','tp_1'}, dimensions={0} | all-to-all | bytes 4194304 | tf_op jit(solution)/shard_map/all_to_all | solution.py:31
  269.7 1.0 reduce_sum.52
  270.7 5.5 %all-to-all-start.2 = ((bf16[32,16,128]{2,1,0:T(8,128)(2,1)}), bf16[32,16,128]{2,1,0:T(8,128)(2,1)S(1)}, u32[]{:S(2)}, u32[]{:S(2)}) async-start(bf16[32,16,128]{2,1,0:T(8,128)(2,1)} %bitcast.12), calls=%async_computation.2 | async-start | bytes 262144 | tf_op jit(solution)/shard_map/all_to_all | solution.py:161
  276.2 0.8 dynamic_slice.10
  277.0 15.4 %all-to-all-done.2 = bf16[32,16,128]{2,1,0:T(8,128)(2,1)S(1)} async-done(((bf16[32,16,128]{2,1,0:T(8,128)(2,1)}), bf16[32,16,128]{2,1,0:T(8,128)(2,1)S(1)}, u32[]{:S(2)}, u32[]{:S(2)}) %all-to-all-start.2) | async-done | bytes 131104 | tf_op jit(solution)/shard_map/all_to_all | solution.py:161
  292.4 0.9 gather_fusion
  293.5 0.9 multiply_reduce_fusion
  294.3 6.6 %psum.14 = f32[128]{0:T(128)S(1)} all-reduce(f32[128]{0:T(128)S(1)} %multiply_reduce_fusion), channel_id=1, replica_groups=mesh['sp'=32,'tp_0'=4,'tp_1'=4] {'tp_0'}, use_global_device_ids=true, to_apply=%region_8.9 | all-reduce | flops 128 | bytes 1024 | tf_op jit(solution)/shard_map/psum | solution.py:37
  300.9 6.7 %psum.15 = f32[128]{0:T(128)S(1)} all-reduce(f32[128]{0:T(128)S(1)} %psum.14), channel_id=1, replica_groups=mesh['sp'=32,'tp_0'=4,'tp_1'=4] {'tp_1'}, use_global_device_ids=true, to_apply=%region_9.10 | all-reduce | flops 128 | bytes 1024 | tf_op jit(solution)/shard_map/psum | solution.py:37
  307.6 0.9 add_convert_fusion.1
  308.6 0.9 broadcast_in_dim.77
  309.5 4.1 all-to-all-start.3
  313.9 0.6 slice.689
  314.5 0.6 slice.698
  315.1 0.6 slice.691
  315.7 0.6 slice.601
  316.3 0.6 slice.602
  316.9 0.6 slice.606
  317.8 4.8 %all-to-all-done.3 = bf16[16,128,128]{1,2,0:T(8,128)(2,1)S(1)} async-done(((bf16[16,128,128]{1,2,0:T(8,128)(2,1)}), bf16[16,128,128]{1,2,0:T(8,128)(2,1)S(1)}, u32[]{:S(2)}, u32[]{:S(2)}) %all-to-all-start.3) | async-done | bytes 524320 | tf_op jit(solution)/shard_map/all_to_all | solution.py:49
  322.8 0.6 slice.695
  323.4 0.6 slice.693
  329.7 0.6 slice.743
  334.9 0.6 pad.214
  335.5 0.6 pad.215
  336.2 0.6 pad.228
  336.8 0.6 pad.229
  337.7 0.7 reshape.170
  338.4 10.1 %all-to-all-start.6 = ((f32[32,1,128]{2,1,0:T(1,128)}), f32[32,1,128]{2,1,0:T(1,128)S(1)}, u32[]{:S(2)}, u32[]{:S(2)}) async-start(f32[32,1,128]{2,1,0:T(1,128)} %reshape.170), calls=%async_computation.6 | async-start | bytes 32768 | tf_op jit(solution)/shard_map/all_to_all | solution.py:49
  348.7 11.5 %all-to-all-done.6 = f32[32,1,128]{2,1,0:T(1,128)S(1)} async-done(((f32[32,1,128]{2,1,0:T(1,128)}), f32[32,1,128]{2,1,0:T(1,128)S(1)}, u32[]{:S(2)}, u32[]{:S(2)}) %all-to-all-start.6) | async-done | bytes 16416 | tf_op jit(solution)/shard_map/all_to_all | solution.py:49
  360.8 0.7 reduce.7
  364.5 0.7 fusion.27
  365.2 0.6 slice.650
  365.8 0.6 slice.604
  366.4 0.6 slice.603
  377.1 0.6 pad.200
  377.7 0.6 pad.201
  378.3 0.6 pad.186
  378.9 0.6 pad.187
  380.0 15.4 %all_to_all.51 = f32[32,1,128]{2,1,0:T(1,128)S(1)} all-to-all(f32[32,1,128]{2,1,0:T(1,128)S(1)} %reshape.166), channel_id=1, replica_groups=mesh['sp'=32,'tp_0'=4,'tp_1'=4] {'sp'}, dimensions={0} | all-to-all | bytes 32768 | tf_op jit(solution)/shard_map/all_to_all | solution.py:49
  395.4 0.7 reduce.8
  400.0 1.1 reshape.168
  401.1 4.7 %all-to-all-start.5 = ((bf16[32,2,2048]{2,1,0:T(2,128)(2,1)}), bf16[32,2,2048]{2,1,0:T(2,128)(2,1)S(1)}, u32[]{:S(2)}, u32[]{:S(2)}) async-start(bf16[32,2,2048]{2,1,0:T(2,128)(2,1)} %reshape.168), calls=%async_computation.5 | async-start | bytes 524288 | tf_op jit(solution)/shard_map/all_to_all | solution.py:31
  405.8 3.3 fusion
  409.1 3.2 fusion.1
  412.3 1.3 fusion.2
  413.6 0.7 fusion.32
  414.3 13.0 %all-to-all-done.5 = bf16[32,2,2048]{2,1,0:T(2,128)(2,1)S(1)} async-done(((bf16[32,2,2048]{2,1,0:T(2,128)(2,1)}), bf16[32,2,2048]{2,1,0:T(2,128)(2,1)S(1)}, u32[]{:S(2)}, u32[]{:S(2)}) %all-to-all-start.5) | async-done | bytes 262176 | tf_op jit(solution)/shard_map/all_to_all | solution.py:31
  427.8 0.7 copy.115
  (313 shorter events, 31.6 us)
Async XLA Ops:
  0.6 229.6 %copy-start = (bf16[1,2048,128]{2,1,0:T(8,128)(2,1)S(1)}, bf16[1,2048,128]{2,1,0:T(8,128)(2,1)}, u32[]{:S(2)}) copy-start(bf16[1,2048,128]{2,1,0:T(8,128)(2,1)} %param.21) | copy-start | bytes 1572868
  0.6 5.9 %copy-start.3 = (bf16[128,2048]{1,0:T(8,128)(2,1)S(1)}, bf16[128,2048]{1,0:T(8,128)(2,1)}, u32[]{:S(2)}) copy-start(bf16[128,2048]{1,0:T(8,128)(2,1)} %param.15) | copy-start | bytes 1572868
  8.9 2.7 copy-start.10
  230.2 2.1 copy-start.1
  230.2 1.4 copy-start.4
  231.6 2.0 copy-start.14
  231.6 1.3 copy-start.12
  233.0 0.7 copy-start.16
  269.7 37.9 %copy-start.11 = (f32[128]{0:T(128)S(1)}, f32[128]{0:T(128)}, u32[]{:S(2)}) copy-start(f32[128]{0:T(128)} %param.17) | copy-start | bytes 1540
  269.7 43.9 %copy-start.13 = (f32[64]{0:T(128)S(1)}, f32[64]{0:T(128)}, u32[]{:S(2)}) copy-start(f32[64]{0:T(128)} %param.27) | copy-start | bytes 772
  269.7 44.0 %copy-start.5 = (f32[128,64]{0,1:T(8,128)S(1)}, f32[128,64]{0,1:T(8,128)}, u32[]{:S(2)}) copy-start(f32[128,64]{0,1:T(8,128)} %param.28) | copy-start | bytes 98308
  269.7 44.0 %copy-start.7 = (bf16[128,64]{0,1:T(8,128)(2,1)S(1)}, bf16[128,64]{0,1:T(8,128)(2,1)}, u32[]{:S(2)}) copy-start(bf16[128,64]{0,1:T(8,128)(2,1)} %param.25) | copy-start | bytes 49156
  270.7 51.9 %copy-start.6 = (bf16[2048,64]{0,1:T(8,128)(2,1)S(1)}, bf16[2048,64]{0,1:T(8,128)(2,1)}, u32[]{:S(2)}) copy-start(bf16[2048,64]{0,1:T(8,128)(2,1)} %param.29) | copy-start | bytes 786436
  270.7 21.7 %all-to-all-start.2 = ((bf16[32,16,128]{2,1,0:T(8,128)(2,1)}), bf16[32,16,128]{2,1,0:T(8,128)(2,1)S(1)}, u32[]{:S(2)}, u32[]{:S(2)}) async-start(bf16[32,16,128]{2,1,0:T(8,128)(2,1)} %bitcast.12), calls=%async_computation.2 | async-start | bytes 262144 | tf_op jit(solution)/shard_map/all_to_all | solution.py:161
  309.5 13.1 %all-to-all-start.3 = ((bf16[16,128,128]{1,2,0:T(8,128)(2,1)}), bf16[16,128,128]{1,2,0:T(8,128)(2,1)S(1)}, u32[]{:S(2)}, u32[]{:S(2)}) async-start(bf16[16,128,128]{1,2,0:T(8,128)(2,1)} %broadcast_in_dim.77), calls=%async_computation.3 | async-start | bytes 1048576 | tf_op jit(solution)/shard_map/all_to_all | solution.py:49
  334.7 29.7 %copy-start.8 = (bf16[128,64]{0,1:T(8,128)(2,1)S(1)}, bf16[128,64]{0,1:T(8,128)(2,1)}, u32[]{:S(2)}) copy-start(bf16[128,64]{0,1:T(8,128)(2,1)} %param.24) | copy-start | bytes 49156
  334.7 29.7 %copy-start.9 = (bf16[128,64]{0,1:T(8,128)(2,1)S(1)}, bf16[128,64]{0,1:T(8,128)(2,1)}, u32[]{:S(2)}) copy-start(bf16[128,64]{0,1:T(8,128)(2,1)} %param.26) | copy-start | bytes 49156
  338.4 21.9 %all-to-all-start.6 = ((f32[32,1,128]{2,1,0:T(1,128)}), f32[32,1,128]{2,1,0:T(1,128)S(1)}, u32[]{:S(2)}, u32[]{:S(2)}) async-start(f32[32,1,128]{2,1,0:T(1,128)} %reshape.170), calls=%async_computation.6 | async-start | bytes 32768 | tf_op jit(solution)/shard_map/all_to_all | solution.py:49
  401.1 26.2 %all-to-all-start.5 = ((bf16[32,2,2048]{2,1,0:T(2,128)(2,1)}), bf16[32,2,2048]{2,1,0:T(2,128)(2,1)S(1)}, u32[]{:S(2)}, u32[]{:S(2)}) async-start(bf16[32,2,2048]{2,1,0:T(2,128)(2,1)} %reshape.168), calls=%async_computation.5 | async-start | bytes 524288 | tf_op jit(solution)/shard_map/all_to_all | solution.py:31
  405.8 6.5 %copy-start.2 = (bf16[32,16,4096]{2,1,0:T(8,128)(2,1)S(1)}, bf16[32,16,4096]{2,1,0:T(8,128)(2,1)}, u32[]{:S(2)}) copy-start(bf16[32,16,4096]{2,1,0:T(8,128)(2,1)} %copy-done.1) | copy-start | bytes 12582916
  409.1 3.2 copy-start.15
  409.1 3.2 copy-start.17
where the time goes:
time: 436 us; the launch traced here: 429 us
  blocking collectives  270 us (62%)
  local copies, waits for them, and re-layouts  57.2 us (13%)
  waiting for transfers between devices  44.7 us (10%)
  starting transfers between devices  24.5 us (6%)
  other arithmetic  17.6 us (4%)
  matrix products  11.9 us (3%)
    all_to_all x1, blocking collectives, side_by_side(): lax.all_to_all(both, axis, split_axis=split_dim, concat_axis=concat_dim,...  207 us
    all_to_all x1, blocking collectives, sum_at_owner(): lax.all_to_all(parts, axis, split_axis=0, concat_axis=0, tiled=True)  34 us
    all_to_all x2, waiting for transfers between devices, sent_to_all(): lax.all_to_all(jnp.broadcast_to(value[None], (count, *value.shape)), axis...  16.4 us
    all_to_all x1, waiting for transfers between devices, shards(): lax.all_to_all(shared, 'sp', split_axis=0, concat_axis=0, tiled=True)  15.4 us
    all_to_all x1, blocking collectives, sent_to_all(): lax.all_to_all(jnp.broadcast_to(value[None], (count, *value.shape)), axis...  15.4 us
    all_to_all x2, starting transfers between devices, sent_to_all(): lax.all_to_all(jnp.broadcast_to(value[None], (count, *value.shape)), axis...  14.2 us
    psum x2, blocking collectives, over_axes(): value = lax.psum(value, axis)  13.3 us
    all_to_all x1, waiting for transfers between devices, sum_at_owner(): lax.all_to_all(parts, axis, split_axis=0, concat_axis=0, tiled=True)  13 us
  transfers between devices with their start and end apart: 4, of which 4 were waited for; matrix products, arithmetic and copies ran while one was open for 3% of the time, Pallas kernels for 0%

commit v1 on v0

--- a/solution.py
+++ b/solution.py
@@ -34,7 +34,7 @@
 
 def over_axes(value, axes):
     for axis in axes:
-        value = lax.psum(value, axis)
+        value = jnp.sum(lax.all_gather(value, axis), axis=0)
     return value
 
 

time: 436 us -> 435 us (level)
    psum x2 -> x0, blocking collectives: 13.3 us -> none  [over_axes(): value = lax.psum(value, axis)]
    all_gather x0 -> x2, blocking collectives: none -> 11.6 us  [over_axes(): value = jnp.sum(lax.all_gather(value, axis), axis=0)]
where the time goes in v1:
time: 435 us; the launch traced here: 427 us
  blocking collectives  268 us (62%)
  local copies, waits for them, and re-layouts  57.2 us (13%)
  waiting for transfers between devices  44.8 us (10%)
  starting transfers between devices  24.7 us (6%)
  other arithmetic  17.7 us (4%)
  matrix products  11.9 us (3%)
    all_to_all x1, blocking collectives, side_by_side(): lax.all_to_all(both, axis, split_axis=split_dim, concat_axis=concat_dim,...  207 us
    all_to_all x1, blocking collectives, sum_at_owner(): lax.all_to_all(parts, axis, split_axis=0, concat_axis=0, tiled=True)  34 us
    all_to_all x2, waiting for transfers between devices, sent_to_all(): lax.all_to_all(jnp.broadcast_to(value[None], (count, *value.shape)), axis...  16.4 us
    all_to_all x1, waiting for transfers between devices, shards(): lax.all_to_all(shared, 'sp', split_axis=0, concat_axis=0, tiled=True)  15.4 us
    all_to_all x1, blocking collectives, sent_to_all(): lax.all_to_all(jnp.broadcast_to(value[None], (count, *value.shape)), axis...  15.4 us
    all_to_all x2, starting transfers between devices, sent_to_all(): lax.all_to_all(jnp.broadcast_to(value[None], (count, *value.shape)), axis...  14.4 us
    all_to_all x1, waiting for transfers between devices, sum_at_owner(): lax.all_to_all(parts, axis, split_axis=0, concat_axis=0, tiled=True)  13 us
    all_gather x2, blocking collectives, over_axes(): value = jnp.sum(lax.all_gather(value, axis), axis=0)  11.6 us
  transfers between devices with their start and end apart: 4, of which 4 were waited for; matrix products, arithmetic and copies ran while one was open for 3% of the time, Pallas kernels for 0%

profile of v1, /device:TPU:1, one launch (start us, length us, event | category | flops | bytes accessed | tf_op | source)
XLA Modules:
  0.0 427.2 jit_solution(8712252438477142159)
XLA Ops:
  0.7 0.8 broadcast_multiply_fusion
  1.4 0.8 copy.99
  3.6 1.7 broadcast_in_dim.73
  5.3 1.2 reshape.157
  6.5 2.4 mul.410
  8.9 2.7 mul.411
  12.0 4.4 %scatter_custom_fusion.1 = bf16[512,2048]{1,0:T(8,128)(2,1)} fusion(s32[256]{0:T(256)S(1)} %bitcast.132, bf16[256,2048]{1,0:T(8,128)(2,1)} %reshape.157, bf16[]{:T(256)} %constant.16.clone.1), kind=kCustom, calls=%fused_computation.27 | custom fusion | bytes 2097664 | tf_op jit(solution)/shard_map/scatter | solution.py:134
  16.4 3.8 scatter_custom_fusion
  20.2 2.7 pad_maximum_fusion
  22.9 207.4 %all_to_all.49 = bf16[32,16,4096]{2,1,0:T(8,128)(2,1)S(1)} all-to-all(bf16[32,16,4096]{2,1,0:T(8,128)(2,1)S(1)} %bitcast.101), channel_id=1, replica_groups=mesh['sp'=32,'tp_0'=4,'tp_1'=4] {'sp'}, dimensions={0} | all-to-all | bytes 8388608 | tf_op jit(solution)/shard_map/all_to_all | solution.py:13
  230.2 0.7 fusion.9
  231.0 0.7 copy-done.4
  231.6 0.7 fusion.11
  233.0 0.7 multiply_convert_fusion.3
  233.7 0.7 fusion.18
  234.4 0.7 fusion.6
  235.7 34.0 %all_to_all.50 = bf16[16,512,128]{2,1,0:T(8,128)(2,1)S(1)} all-to-all(bf16[16,512,128]{2,1,0:T(8,128)(2,1)S(1)} %bitcast.102), channel_id=1, replica_groups=mesh['sp'=32,'tp_0'=4,'tp_1'=4] {'tp_0','tp_1'}, dimensions={0} | all-to-all | bytes 4194304 | tf_op jit(solution)/shard_map/all_to_all | solution.py:31
  269.7 1.0 reduce_sum.70
  270.7 5.5 %all-to-all-start.2 = ((bf16[32,16,128]{2,1,0:T(8,128)(2,1)}), bf16[32,16,128]{2,1,0:T(8,128)(2,1)S(1)}, u32[]{:S(2)}, u32[]{:S(2)}) async-start(bf16[32,16,128]{2,1,0:T(8,128)(2,1)} %bitcast.12), calls=%async_computation.2 | async-start | bytes 262144 | tf_op jit(solution)/shard_map/all_to_all | solution.py:161
  276.2 0.8 dynamic_slice.10
  277.0 15.4 %all-to-all-done.2 = bf16[32,16,128]{2,1,0:T(8,128)(2,1)S(1)} async-done(((bf16[32,16,128]{2,1,0:T(8,128)(2,1)}), bf16[32,16,128]{2,1,0:T(8,128)(2,1)S(1)}, u32[]{:S(2)}, u32[]{:S(2)}) %all-to-all-start.2) | async-done | bytes 131104 | tf_op jit(solution)/shard_map/all_to_all | solution.py:161
  292.4 0.9 gather_fusion
  293.5 0.9 multiply_reduce_fusion
  294.3 5.8 %all-gather.2 = f32[4,1,128]{2,1,0:T(1,128)S(1)} all-gather(f32[1,1,128]{2,1,0:T(1,128)S(1)} %bitcast.136), channel_id=2, replica_groups=mesh['sp'=32,'tp_0'=4,'tp_1'=4] {'tp_0'}, dimensions={0}, use_global_device_ids=true | all-gather | bytes 2560 | tf_op jit(solution)/shard_map/all_gather | solution.py:37
  300.2 5.8 %all-gather.3 = f32[4,1,128]{2,1,0:T(1,128)S(1)} all-gather(f32[1,1,128]{2,1,0:T(1,128)S(1)} %bitcast.137), channel_id=3, replica_groups=mesh['sp'=32,'tp_0'=4,'tp_1'=4] {'tp_1'}, dimensions={0}, use_global_device_ids=true | all-gather | bytes 2560 | tf_op jit(solution)/shard_map/all_gather | solution.py:37
  306.0 0.9 add_convert_fusion.1
  307.0 0.9 broadcast_in_dim.77
  307.9 4.1 all-to-all-start.3
  312.3 0.6 slice.689
  312.9 0.6 slice.698
  313.5 0.6 slice.691
  314.1 0.6 slice.601
  314.7 0.6 slice.602
  315.3 0.6 slice.606
  316.1 4.8 %all-to-all-done.3 = bf16[16,128,128]{1,2,0:T(8,128)(2,1)S(1)} async-done(((bf16[16,128,128]{1,2,0:T(8,128)(2,1)}), bf16[16,128,128]{1,2,0:T(8,128)(2,1)S(1)}, u32[]{:S(2)}, u32[]{:S(2)}) %all-to-all-start.3) | async-done | bytes 524320 | tf_op jit(solution)/shard_map/all_to_all | solution.py:49
  321.2 0.6 slice.695
  321.8 0.6 slice.693
  328.0 0.6 slice.743
  333.3 0.6 pad.214
  333.9 0.6 pad.215
  334.5 0.6 pad.228
  335.2 0.6 pad.229
  336.1 0.7 reshape.180
  336.8 10.3 %all-to-all-start.6 = ((f32[32,1,128]{2,1,0:T(1,128)}), f32[32,1,128]{2,1,0:T(1,128)S(1)}, u32[]{:S(2)}, u32[]{:S(2)}) async-start(f32[32,1,128]{2,1,0:T(1,128)} %reshape.180), calls=%async_computation.6 | async-start | bytes 32768 | tf_op jit(solution)/shard_map/all_to_all | solution.py:49
  347.2 11.5 %all-to-all-done.6 = f32[32,1,128]{2,1,0:T(1,128)S(1)} async-done(((f32[32,1,128]{2,1,0:T(1,128)}), f32[32,1,128]{2,1,0:T(1,128)S(1)}, u32[]{:S(2)}, u32[]{:S(2)}) %all-to-all-start.6) | async-done | bytes 16416 | tf_op jit(solution)/shard_map/all_to_all | solution.py:49
  359.3 0.7 reduce.9
  363.0 0.7 fusion.27
  363.7 0.6 slice.650
  364.3 0.6 slice.604
  364.9 0.6 slice.603
  375.6 0.6 pad.200
  376.2 0.6 pad.201
  376.9 0.6 pad.186
  377.5 0.6 pad.187
  378.6 15.4 %all_to_all.51 = f32[32,1,128]{2,1,0:T(1,128)S(1)} all-to-all(f32[32,1,128]{2,1,0:T(1,128)S(1)} %reshape.176), channel_id=1, replica_groups=mesh['sp'=32,'tp_0'=4,'tp_1'=4] {'sp'}, dimensions={0} | all-to-all | bytes 32768 | tf_op jit(solution)/shard_map/all_to_all | solution.py:49
  394.0 0.7 reduce.10
  398.5 1.1 reshape.178
  399.6 4.7 %all-to-all-start.5 = ((bf16[32,2,2048]{2,1,0:T(2,128)(2,1)}), bf16[32,2,2048]{2,1,0:T(2,128)(2,1)S(1)}, u32[]{:S(2)}, u32[]{:S(2)}) async-start(bf16[32,2,2048]{2,1,0:T(2,128)(2,1)} %reshape.178), calls=%async_computation.5 | async-start | bytes 524288 | tf_op jit(solution)/shard_map/all_to_all | solution.py:31
  404.3 3.3 fusion
  407.6 3.2 fusion.1
  410.9 1.3 fusion.2
  412.2 0.7 fusion.32
  412.9 13.0 %all-to-all-done.5 = bf16[32,2,2048]{2,1,0:T(2,128)(2,1)S(1)} async-done(((bf16[32,2,2048]{2,1,0:T(2,128)(2,1)}), bf16[32,2,2048]{2,1,0:T(2,128)(2,1)S(1)}, u32[]{:S(2)}, u32[]{:S(2)}) %all-to-all-start.5) | async-done | bytes 262176 | tf_op jit(solution)/shard_map/all_to_all | solution.py:31
  426.3 0.7 copy.115
  (315 shorter events, 31.6 us)
Async XLA Ops:
  0.6 229.6 %copy-start = (bf16[1,2048,128]{2,1,0:T(8,128)(2,1)S(1)}, bf16[1,2048,128]{2,1,0:T(8,128)(2,1)}, u32[]{:S(2)}) copy-start(bf16[1,2048,128]{2,1,0:T(8,128)(2,1)} %param.21) | copy-start | bytes 1572868
  0.6 5.9 %copy-start.3 = (bf16[128,2048]{1,0:T(8,128)(2,1)S(1)}, bf16[128,2048]{1,0:T(8,128)(2,1)}, u32[]{:S(2)}) copy-start(bf16[128,2048]{1,0:T(8,128)(2,1)} %param.15) | copy-start | bytes 1572868
  8.9 2.7 copy-start.10
  230.2 2.1 copy-start.1
  230.2 1.4 copy-start.4
  231.6 2.0 copy-start.14
  231.6 1.3 copy-start.12
  233.0 0.7 copy-start.16
  269.7 36.3 %copy-start.11 = (f32[128]{0:T(128)S(1)}, f32[128]{0:T(128)}, u32[]{:S(2)}) copy-start(f32[128]{0:T(128)} %param.17) | copy-start | bytes 1540
  269.7 42.3 %copy-start.13 = (f32[64]{0:T(128)S(1)}, f32[64]{0:T(128)}, u32[]{:S(2)}) copy-start(f32[64]{0:T(128)} %param.27) | copy-start | bytes 772
  269.7 42.4 %copy-start.5 = (f32[128,64]{0,1:T(8,128)S(1)}, f32[128,64]{0,1:T(8,128)}, u32[]{:S(2)}) copy-start(f32[128,64]{0,1:T(8,128)} %param.28) | copy-start | bytes 98308
  269.7 42.4 %copy-start.7 = (bf16[128,64]{0,1:T(8,128)(2,1)S(1)}, bf16[128,64]{0,1:T(8,128)(2,1)}, u32[]{:S(2)}) copy-start(bf16[128,64]{0,1:T(8,128)(2,1)} %param.25) | copy-start | bytes 49156
  270.7 50.3 %copy-start.6 = (bf16[2048,64]{0,1:T(8,128)(2,1)S(1)}, bf16[2048,64]{0,1:T(8,128)(2,1)}, u32[]{:S(2)}) copy-start(bf16[2048,64]{0,1:T(8,128)(2,1)} %param.29) | copy-start | bytes 786436
  270.7 21.7 %all-to-all-start.2 = ((bf16[32,16,128]{2,1,0:T(8,128)(2,1)}), bf16[32,16,128]{2,1,0:T(8,128)(2,1)S(1)}, u32[]{:S(2)}, u32[]{:S(2)}) async-start(bf16[32,16,128]{2,1,0:T(8,128)(2,1)} %bitcast.12), calls=%async_computation.2 | async-start | bytes 262144 | tf_op jit(solution)/shard_map/all_to_all | solution.py:161
  307.9 13.1 %all-to-all-start.3 = ((bf16[16,128,128]{1,2,0:T(8,128)(2,1)}), bf16[16,128,128]{1,2,0:T(8,128)(2,1)S(1)}, u32[]{:S(2)}, u32[]{:S(2)}) async-start(bf16[16,128,128]{1,2,0:T(8,128)(2,1)} %broadcast_in_dim.77), calls=%async_computation.3 | async-start | bytes 1048576 | tf_op jit(solution)/shard_map/all_to_all | solution.py:49
  333.1 29.9 %copy-start.8 = (bf16[128,64]{0,1:T(8,128)(2,1)S(1)}, bf16[128,64]{0,1:T(8,128)(2,1)}, u32[]{:S(2)}) copy-start(bf16[128,64]{0,1:T(8,128)(2,1)} %param.24) | copy-start | bytes 49156
  333.1 29.9 %copy-start.9 = (bf16[128,64]{0,1:T(8,128)(2,1)S(1)}, bf16[128,64]{0,1:T(8,128)(2,1)}, u32[]{:S(2)}) copy-start(bf16[128,64]{0,1:T(8,128)(2,1)} %param.26) | copy-start | bytes 49156
  336.8 22.0 %all-to-all-start.6 = ((f32[32,1,128]{2,1,0:T(1,128)}), f32[32,1,128]{2,1,0:T(1,128)S(1)}, u32[]{:S(2)}, u32[]{:S(2)}) async-start(f32[32,1,128]{2,1,0:T(1,128)} %reshape.180), calls=%async_computation.6 | async-start | bytes 32768 | tf_op jit(solution)/shard_map/all_to_all | solution.py:49
  399.6 26.3 %all-to-all-start.5 = ((bf16[32,2,2048]{2,1,0:T(2,128)(2,1)}), bf16[32,2,2048]{2,1,0:T(2,128)(2,1)S(1)}, u32[]{:S(2)}, u32[]{:S(2)}) async-start(bf16[32,2,2048]{2,1,0:T(2,128)(2,1)} %reshape.178), calls=%async_computation.5 | async-start | bytes 524288 | tf_op jit(solution)/shard_map/all_to_all | solution.py:31
  404.3 6.5 %copy-start.2 = (bf16[32,16,4096]{2,1,0:T(8,128)(2,1)S(1)}, bf16[32,16,4096]{2,1,0:T(8,128)(2,1)}, u32[]{:S(2)}) copy-start(bf16[32,16,4096]{2,1,0:T(8,128)(2,1)} %copy-done.1) | copy-start | bytes 12582916
  407.6 3.2 copy-start.15
  407.6 3.2 copy-start.17
